TPU v7x, 512 devices: a whole 4x8x8 slice. The times are simulated.
512 devices in a mesh: kv: 64 (over z, y), tp: 8 (over x, core).
Axes of the slice: x: 4, y: 8, z: 8, core: 2. Of those that a mesh axis runs over, the one named last changes fastest.
Arguments:
- hidden_in: bfloat16 [8, 1024], P(None, 'tp'), may hold values from -18 to 18, as said below
- input_gain: float32 [1024], P('tp'), may hold values from 0.1 to 1.9
- down_query: bfloat16 [1024, 256], P('tp'), may hold values from -0.1875 to 0.1875
- down_latent: bfloat16 [1024, 256], P('tp'), may hold values from -0.1875 to 0.1875
- down_rope: bfloat16 [1024, 64], P('tp'), may hold values from -0.1875 to 0.1875
- query_gain: float32 [256], replicated, may hold values from 0.1 to 1.9
- latent_gain: float32 [256], replicated, may hold values from 0.1 to 1.9
- up_query: bfloat16 [256, 8, 128], P(None, 'tp'), may hold values from -0.375 to 0.375
- up_rope: bfloat16 [256, 8, 64], P(None, 'tp'), may hold values from -0.375 to 0.375
- key_up: bfloat16 [256, 8, 128], P(None, 'tp'), may hold values from -0.375 to 0.375
- value_up: bfloat16 [256, 8, 128], P(None, 'tp'), may hold values from -0.375 to 0.375
- out_proj: bfloat16 [1024, 1024], P('tp', 'kv'), may hold values from -2 to 2, as said below
- output_gain: float32 [1024], P('kv'), may hold values from 0.1 to 1.9
- latent_cache: bfloat16 [8, 65536, 256], P(None, ('kv', 'tp')), may hold values from -6 to 6
- rope_cache: bfloat16 [8, 65536, 64], P(None, ('kv', 'tp')), may hold values from -6 to 6
- lengths: int32 [8], replicated, may hold values from 1 to 65536, as said below
Outputs:
- mixed: bfloat16 [8, 1024], P(None, 'kv')
Inputs may be any that keep to these rules, and one draw needn't show every extreme that they name: Each length lies between 1 and 65536; in every draw some sequence has exactly 65536 and some exactly 1; lengths are heavily skewed toward short ones. `hidden_in`: activations whose size differs strongly between blocks of 64 features, by sequence. `out_proj`: output projection whose columns differ strongly in size.
All inputs are finite; a program needn't handle non-finite values.
Results may differ from a plain program's by a relative error of at most 0.015.
Values may be sent and summed in bfloat16 or wider, within the bound.
A program may use at most 128 MiB of HBM per device.

v0:
```python
import functools
import math

import jax
import jax.numpy as jnp
import numpy as np
from jax import lax
from jax.experimental import pallas as pl
from jax.experimental.pallas import tpu as pltpu
from jax.sharding import PartitionSpec as P

THETA = 10000.0
EPSILON = 1e-06
MESH = pl.DeviceIdType.MESH
F32 = jnp.float32
BF16 = jnp.bfloat16
NT = (((1,), (1,)), ((), ()))


def iota(shape, dim):
    return lax.broadcasted_iota(jnp.int32, shape, dim)


def dot(a, b):
    return jnp.dot(a, b, preferred_element_type=F32)


def dot_nt(a, b):
    return lax.dot_general(a, b, NT, preferred_element_type=F32)


def sin_cos(x):
    turns = jnp.floor(x * (1.0 / (2 * math.pi)) + 0.5)
    r = (x - turns * 6.28125) - turns * (2 * math.pi - 6.28125)
    r2 = r * r
    s = jnp.full_like(x, 1.0)
    for n in (15, 13, 11, 9, 7, 5, 3):
        s = 1.0 - s * r2 * (1.0 / (n * (n - 1)))
    c = jnp.full_like(x, 1.0)
    for n in (18, 16, 14, 12, 10, 8, 6, 4, 2):
        c = 1.0 - c * r2 * (1.0 / (n * (n - 1)))
    return s * r, c


def turn(v, cosine, sine):
    half = v.shape[-1] // 2
    swapped = jnp.concatenate([-v[:, half:], v[:, :half]], axis=1)
    return v * cosine + swapped * sine


def normed(v, gain):
    return v * lax.rsqrt(jnp.mean(v * v, axis=-1, keepdims=True) + EPSILON) * gain


def kernel(
    K,
    T,
    lengths_h,
    inverse_h,
    hidden_h,
    gain_h,
    dq_h,
    dl_h,
    dr_h,
    qg_h,
    lg_h,
    uq_h,
    ur_h,
    ku_h,
    vu_h,
    op_h,
    lat_h,
    rope_h,
    out,
    hidden,
    gain,
    dq,
    dl,
    dr,
    qg,
    lg,
    uq,
    ur,
    ku,
    vu,
    lat,
    rope,
    rx1,
    rx2,
    rxp,
    tx3,
    rx3,
    tx4,
    rx4,
    rx6,
    spread,
    lengths,
    inverse,
    load_sem,
    s1,
    r1,
    s2,
    r2,
    sp,
    rp,
    s3,
    r3,
    s4,
    r4,
    s6,
    r6,
):
    N = K * T
    B = hidden.shape[0]
    width = hidden.shape[1] * T
    QR = dq.shape[1]
    KR = dl.shape[1]
    DR = dr.shape[0]
    Hd = uq.shape[0] // QR
    H = Hd * T
    DN = uq.shape[1]
    span = lat.shape[1]
    rows = rx3.shape[1]
    owners = tx3.shape[0]
    k = lax.axis_index("kv")
    t = lax.axis_index("tp")
    me = k * T + t
    factor = 1.0 / math.sqrt(DN + DR)

    def slot_of(kk, tt):
        first = kk * rows
        return lax.div(lax.div(first, Hd) * H + tt * Hd + lax.rem(first, Hd), rows)

    everyone_owns = owners == N

    def if_owner(kk, fn):
        if everyone_owns:
            fn()
        else:
            pl.when(kk * T * rows < B * H)(fn)

    barrier = pltpu.get_barrier_semaphore()

    def to_all(fn):
        def chip(i, carry):
            kk = k + i
            kk = jnp.where(kk >= K, kk - K, kk)
            for tt in range(T):
                fn(kk, tt)
            return carry

        lax.fori_loop(K // 2, K, chip, 0)
        lax.fori_loop(1, K // 2, chip, 0)
        for i in range(1, T):
            fn(k, lax.rem(t + i, T))

    to_all(lambda kk, tt: pl.semaphore_signal(barrier, inc=1, device_id=(kk, tt), device_id_type=MESH))

    pairs = (
        (hidden_h, hidden), (gain_h, gain), (dq_h, dq), (dl_h, dl), (dr_h, dr),
        (uq_h, uq), (ur_h, ur), (ku_h, ku), (qg_h, qg), (lg_h, lg),
        (op_h, rxp.at[t]), (lat_h, lat), (rope_h, rope), (vu_h, vu),
        (lengths_h, lengths), (inverse_h, inverse),
    )
    loads = [pltpu.make_async_copy(a, b, load_sem.at[i]) for i, (a, b) in enumerate(pairs)]
    for load in loads:
        load.start()

    spread[...] = jnp.where(
        lax.div(iota((QR, QR * Hd), 1), Hd) == iota((QR, QR * Hd), 0), 1.0, 0.0
    ).astype(BF16)
    own_rows = iota((B * H, QR * Hd), 0)
    own_mask = (lax.rem(own_rows, H) - t * Hd) == lax.rem(iota((B * H, QR * Hd), 1), Hd)

    def angles(n, per):
        row = lax.div(iota((n, DR), 0), per)
        position = jnp.zeros((n, DR), F32)
        for b in range(B):
            position = jnp.where(row == b, lengths[b].astype(F32), position)
        return sin_cos(position * inverse[...])

    for load in loads[:5]:
        load.wait()
    floats = hidden[...].astype(F32)
    scaled = (floats * gain[...]).astype(BF16)
    low = rx1.at[t]
    low[:, :QR] = dot(scaled, dq[...])
    low[:, QR : QR + KR] = dot(scaled, dl[...])
    low[:, QR + KR : QR + KR + DR] = dot_nt(scaled, dr[...])
    low[:, QR + KR + DR :] = jnp.broadcast_to(
        jnp.sum(floats * floats, axis=1, keepdims=True), (B, rx1.shape[2] - QR - KR - DR)
    )
    for load in loads[-2:]:
        load.wait()
    sine8, cosine8 = angles(B, 1)
    sine_all, cosine_all = angles(B * H, H)
    pl.semaphore_wait(barrier, N - 1)

    def swap(buffer, send, recv):
        copies = []
        for i in range(1, T):
            peer = lax.rem(t + i, T)
            copies.append(
                pltpu.make_async_remote_copy(
                    src_ref=buffer.at[t],
                    dst_ref=buffer.at[t],
                    send_sem=send.at[i],
                    recv_sem=recv.at[i],
                    device_id=(k, peer),
                    device_id_type=MESH,
                )
            )
        for copy in copies:
            copy.start()
        return copies

    copies1 = swap(rx1, s1, r1)
    for load in loads[5:-2]:
        load.wait()
    for copy in copies1:
        copy.wait()
    total = rx1[0]
    for i in range(1, T):
        total = total + rx1[i]
    inv_rms = lax.rsqrt(total[:, QR + KR + DR : QR + KR + DR + 1] / width + EPSILON)
    total = total * inv_rms
    query_normed = normed(total[:, :QR], qg[...]).astype(BF16)
    latent_new = normed(total[:, QR : QR + KR], lg[...]).astype(BF16).astype(F32)
    rope_new = turn(total[:, QR + KR : QR + KR + DR], cosine8, sine8).astype(BF16).astype(F32)

    wide = dot(query_normed, spread[...])
    wide = jnp.concatenate(
        [jnp.broadcast_to(wide[b : b + 1, :], (H, QR * Hd)) for b in range(B)], axis=0
    )
    wide = jnp.where(own_mask, wide, 0.0).astype(BF16)
    query_nope = dot(wide, uq[...]).astype(BF16)
    roped = dot_nt(query_normed, ur[...])
    roped = jnp.concatenate(
        [jnp.broadcast_to(roped[b : b + 1, :], (H, Hd * DR)) for b in range(B)], axis=0
    )
    head = lax.rem(iota((B * H, DR), 0), H) - t * Hd
    query_rope = jnp.zeros((B * H, DR), F32)
    for h in range(Hd):
        query_rope = jnp.where(head == h, roped[:, h * DR : (h + 1) * DR], query_rope)
    query_rope = turn(query_rope, cosine_all, sine_all)
    tall = jnp.where(own_mask, dot_nt(query_nope, ku[...]), 0.0).astype(BF16)
    queries = rx2.at[t]
    queries[:, :KR] = dot_nt(tall, spread[...]).astype(BF16)
    queries[:, KR : KR + DR] = query_rope.astype(BF16)
    queries[:, KR + DR :] = jnp.zeros((B * H, rx2.shape[2] - KR - DR), BF16)
    copies2 = swap(rx2, s2, r2)
    copies_p = swap(rxp, sp, rp)
    for copy in copies2:
        copy.wait()
    query = rx2[0].astype(F32)
    for i in range(1, T):
        query = query + rx2[i].astype(F32)

    offset = me * span
    lane = iota((H, span), 1) + offset
    mark = iota((H, 128), 1)
    first = me == 0
    for b in range(B):
        q = query[b * H : (b + 1) * H]
        qb = q.astype(BF16)
        usable = lane < lengths[b]
        scores = (
            dot_nt(qb[:, :KR], lat[b]) + dot(qb[:, KR : KR + DR], rope[b])
        ) * factor
        scores = jnp.where(usable, scores, -1e30)
        new_score = (
            jnp.sum(q[:, :KR] * latent_new[b : b + 1], axis=1, keepdims=True)
            + jnp.sum(q[:, KR : KR + DR] * rope_new[b : b + 1], axis=1, keepdims=True)
        ) * factor
        new_score = jnp.where(first, new_score, -1e30)
        top = jnp.maximum(jnp.max(scores, axis=1, keepdims=True), new_score)
        weights = jnp.where(usable, jnp.exp(scores - top), 0.0)
        fresh = jnp.where(first, jnp.exp(new_score - top), 0.0)
        mass = jnp.sum(weights, axis=1, keepdims=True) + fresh
        summed = dot(weights.astype(BF16), lat[b]) + fresh * latent_new[b : b + 1]
        high = top.astype(BF16).astype(F32)
        middle = (top - high).astype(BF16).astype(F32)
        small = ((top - high) - middle).astype(BF16).astype(F32)
        mass_high = mass.astype(BF16).astype(F32)
        tail = jnp.where(
            mark == 0,
            high,
            jnp.where(
                mark == 1,
                middle,
                jnp.where(mark == 2, small, jnp.where(mark == 3, mass_high, mass - mass_high)),
            ),
        )
        block = jnp.concatenate([summed, tail], axis=1).astype(BF16)
        for j in range(H // rows):
            tx3[b * (H // rows) + j] = block[j * rows : (j + 1) * rows]

    def part(kk, tt):
        return pltpu.make_async_remote_copy(
            src_ref=tx3.at[slot_of(kk, tt)],
            dst_ref=rx3.at[me],
            send_sem=s3,
            recv_sem=r3,
            device_id=(kk, tt),
            device_id_type=MESH,
        )

    to_all(lambda kk, tt: if_owner(kk, lambda: part(kk, tt).start()))

    mine = slot_of(k, t)

    def values(kk, tt):
        return pltpu.make_async_remote_copy(
            src_ref=tx4,
            dst_ref=rx4.at[mine],
            send_sem=s4,
            recv_sem=r4,
            device_id=(kk, tt),
            device_id_type=MESH,
        )

    def own():
        rx3[me] = tx3[mine]
        pltpu.make_async_copy(rx3.at[pl.ds(0, N - 1)], rx3.at[pl.ds(0, N - 1)], r3).wait()
        parts = rx3[...].astype(F32)
        tail = parts[:, :, KR : KR + 128]
        top = tail[:, :, 0:1] + tail[:, :, 1:2] + tail[:, :, 2:3]
        highest = jnp.max(top, axis=0, keepdims=True)
        scale = jnp.exp(top - highest)
        mass = jnp.sum((tail[:, :, 3:4] + tail[:, :, 4:5]) * scale, axis=0)
        attended = jnp.sum(parts[:, :, :KR] * scale, axis=0) / mass
        attended = jnp.concatenate([attended, jnp.zeros((8 - rows, KR), F32)], axis=0)
        wide = dot(attended.astype(BF16), spread[...])
        head = lax.rem(k * rows + iota((8, KR * Hd), 0), Hd)
        wide = jnp.where(head == lax.rem(iota((8, KR * Hd), 1), Hd), wide, 0.0).astype(BF16)
        value = dot(wide, vu[...])[:rows].astype(BF16)
        tx4[...] = value
        rx4[mine] = value

        to_all(lambda kk, tt: values(kk, tt).start())

    if_owner(k, own)
    for copy in copies_p:
        copy.wait()

    def arrived(n):
        pltpu.make_async_copy(rx4.at[pl.ds(0, n)], rx4.at[pl.ds(0, n)], r4).wait()

    if everyone_owns:
        arrived(owners - 1)
    else:
        owner = k * T * rows < B * H
        pl.when(owner)(lambda: arrived(owners - 1))
        pl.when(jnp.logical_not(owner))(lambda: arrived(owners))

    gathered = rx4[...].astype(F32).reshape(B, H, rx4.shape[2]).astype(BF16)
    out_cols = jnp.zeros(out.shape, F32)
    for i in range(T):
        flat = jnp.concatenate([gathered[:, i * Hd + h, :] for h in range(Hd)], axis=1)
        out_cols = out_cols + dot_nt(flat, rxp[i])
    squares = jnp.sum(out_cols * out_cols, axis=1, keepdims=True)
    diagonal = iota((B, 128), 0) == iota((B, 128), 1)
    rx6[k] = jnp.sum(jnp.where(diagonal, squares, 0.0), axis=0, keepdims=True)

    def norm_part(i):
        return pltpu.make_async_remote_copy(
            src_ref=rx6.at[k],
            dst_ref=rx6.at[k],
            send_sem=s6,
            recv_sem=r6,
            device_id=(lax.rem(k + i, K), t),
            device_id_type=MESH,
        )

    def send6(i, carry):
        norm_part(i).start()
        return carry

    lax.fori_loop(1, K, send6, 0)

    def left(buffer, n, sem):
        pltpu.make_async_copy(buffer.at[pl.ds(0, n)], buffer.at[pl.ds(0, n)], sem).wait()

    if everyone_owns:
        left(rx3, N - 1, s3)
        left(rx4, N - 1, s4)
    else:
        to_all(lambda kk, tt: if_owner(kk, lambda: part(kk, tt).wait_send()))
        if_owner(k, lambda: to_all(lambda kk, tt: values(kk, tt).wait_send()))

    pltpu.make_async_copy(rx6.at[pl.ds(0, K - 1)], rx6.at[pl.ds(0, K - 1)], r6).wait()
    total = jnp.sum(rx6[...], axis=0)
    squares = jnp.sum(
        jnp.where(diagonal, jnp.broadcast_to(total, (B, 128)), 0.0), axis=1, keepdims=True
    )
    out[...] = out_cols * lax.rsqrt(squares / width + EPSILON)
    left(rx6, K - 1, s6)


def shards(
    K, T, hidden_in, input_gain, down_query, down_latent, down_rope, query_gain, latent_gain,
    up_query, up_rope, key_up, value_up, out_proj, output_gain, latent_cache, rope_cache, lengths,
):
    B = hidden_in.shape[0]
    QR, Hd, DN = up_query.shape
    KR, DR, DV = key_up.shape[0], up_rope.shape[2], value_up.shape[2]
    H, N = Hd * T, K * T
    rows = max(1, B * Hd // K)
    owners = B * H // rows
    steps = np.arange(0, DR, 2, dtype=np.float64) / DR
    inverse = np.tile((1.0 / THETA**steps).astype(np.float32), 2)[None, :]
    flat = lambda w: w.reshape(w.shape[0] * w.shape[1], w.shape[2])
    row = lambda v: v.reshape(1, v.shape[0])
    arrays = (
        hidden_in, row(input_gain), down_query, down_latent, down_rope.T, row(query_gain),
        row(latent_gain), flat(up_query), flat(up_rope.transpose(1, 2, 0)), flat(key_up),
        flat(value_up), out_proj.T, latent_cache, rope_cache.transpose(0, 2, 1),
    )
    vm = lambda a: pltpu.VMEM(a.shape, a.dtype)
    local = [vm(a) for i, a in enumerate(arrays) if i != 11]
    low = -(-(QR + KR + DR + 1) // 128) * 128
    wide = -(-(KR + DR) // 128) * 128
    dma = pltpu.SemaphoreType.DMA
    scratch = local + [
        pltpu.VMEM((T, B, low), F32),
        pltpu.VMEM((T, B * H, wide), BF16),
        pltpu.VMEM((T,) + out_proj.shape[::-1], BF16),
        pltpu.VMEM((owners, rows, KR + 128), BF16),
        pltpu.VMEM((N, rows, KR + 128), BF16),
        pltpu.VMEM((rows, DV), BF16),
        pltpu.VMEM((owners, rows, DV), BF16),
        pltpu.VMEM((K, 1, 128), F32),
        pltpu.VMEM((QR, QR * Hd), BF16),
        pltpu.SMEM(lengths.shape, lengths.dtype),
        pltpu.VMEM(inverse.shape, F32),
        dma((len(arrays) + 2,)),
        dma((T,)), dma((T,)), dma((T,)), dma((T,)), dma((T,)), dma((T,)),
        dma, dma, dma, dma, dma, dma,
    ]
    normal = pl.pallas_call(
        functools.partial(kernel, K, T),
        out_shape=jax.ShapeDtypeStruct((B, out_proj.shape[1]), F32),
        in_specs=[pl.BlockSpec(memory_space=pl.ANY)] * (len(arrays) + 2),
        out_specs=pl.BlockSpec(memory_space=pltpu.VMEM),
        scratch_shapes=scratch,
        compiler_params=pltpu.CompilerParams(collective_id=0, has_side_effects=True),
    )(lengths, jnp.asarray(inverse), *arrays)
    return (normal * row(output_gain)).astype(BF16)


def solution(mesh):
    in_specs = (
        P(None, "tp"),
        P("tp"),
        P("tp", None),
        P("tp", None),
        P("tp", None),
        P(),
        P(),
        P(None, "tp", None),
        P(None, "tp", None),
        P(None, "tp", None),
        P(None, "tp", None),
        P("tp", "kv"),
        P("kv"),
        P(None, ("kv", "tp"), None),
        P(None, ("kv", "tp"), None),
        P(),
    )
    body = functools.partial(shards, mesh.shape["kv"], mesh.shape["tp"])
    return jax.shard_map(body, mesh=mesh, in_specs=in_specs, out_specs=P(None, "kv"), check_vma=False)
```

profile of v0, /device:TPU:1, one launch (start us, length us, event | category | flops | bytes accessed | tf_op | source)
XLA Modules:
  0.0 79.7 jit_solution(7030060698427072403)
XLA Ops:
  0.0 0.0 copy-start
  0.0 78.4 %shard_map.163 = f32[8,16]{1,0:T(8,128)} custom-call(s32[8]{0:T(128)} %lengths_h.1, f32[1,64]{1,0:T(1,128)} %constant.2.clone.inverse_h, bf16[8,128]{1,0:T(8,128)(2,1)} %hidden_h.1, f32[1,128]{1,0:T(1,128)} %bitcast.21, bf16[128,256]{1,0:T(8,128)(2,1)} %dq_h.1, bf16[128,256]{1,0:T(8,128)(2,1)} %dl_h.1, bf16[64,128]{1,0:T(8,128)(2,1)} %bitcast.17, ...), custom_call_target="tpu_custom_call" | custom-call | tf_op jit(solution)/shard_map/pallas_call | solution.py:440
  78.4 0.0 copy-done
  78.4 1.3 %multiply_convert_fusion = bf16[8,16]{1,0:T(8,128)(2,1)} fusion(f32[8,16]{1,0:T(8,128)} %shard_map.163, f32[16]{0:T(128)S(1)} %copy-done), kind=kLoop, calls=%fused_computation | loop fusion | flops 256 | bytes 832 | tf_op jit(solution)/shard_map/convert_element_type | solution.py:448
Async XLA Ops:
  0.0 78.4 %copy-start = (f32[16]{0:T(128)S(1)}, f32[16]{0:T(128)}, u32[]{:S(2)}) copy-start(f32[16]{0:T(128)} %param.29) | copy-start | bytes 196
where the time goes:
time: 79.8 us; the launch traced here: 79.7 us
  Pallas kernels  78.4 us (98%)
  other arithmetic  1.25 us (2%)
    pallas_call x1, Pallas kernels, shards(): pl.pallas_call(functools.partial(kernel, K, T), out_shape=jax.ShapeDtypeS...  78.4 us

commit v1 on v0

v1 whole, which is shorter than its diff:
```python
import functools
import math

import jax
import jax.numpy as jnp
import numpy as np
from jax import lax
from jax.experimental import pallas as pl
from jax.experimental.pallas import tpu as pltpu
from jax.sharding import PartitionSpec as P

THETA = 10000.0
EPSILON = 1e-06
MESH = pl.DeviceIdType.MESH
F32 = jnp.float32
BF16 = jnp.bfloat16
NT = (((1,), (1,)), ((), ()))
Y = 8
RING = (4, 3, 5, 2, 6, 1, 7)


def iota(shape, dim):
    return lax.broadcasted_iota(jnp.int32, shape, dim)


def dot(a, b):
    return jnp.dot(a, b, preferred_element_type=F32)


def dot_nt(a, b):
    return lax.dot_general(a, b, NT, preferred_element_type=F32)


def sin_cos(x):
    turns = jnp.floor(x * (1.0 / (2 * math.pi)) + 0.5)
    r = (x - turns * 6.28125) - turns * (2 * math.pi - 6.28125)
    r2 = r * r
    s = jnp.full_like(x, 1.0)
    for n in (15, 13, 11, 9, 7, 5, 3):
        s = 1.0 - s * r2 * (1.0 / (n * (n - 1)))
    c = jnp.full_like(x, 1.0)
    for n in (18, 16, 14, 12, 10, 8, 6, 4, 2):
        c = 1.0 - c * r2 * (1.0 / (n * (n - 1)))
    return s * r, c


def kernel(
    K,
    T,
    lengths_h,
    inverse_h,
    hidden_h,
    gain_h,
    dq_h,
    dl_h,
    dr_h,
    qg_h,
    lg_h,
    uq_h,
    ur_h,
    ku_h,
    vu_h,
    op_h,
    lat_h,
    rope_h,
    out,
    hidden,
    gain,
    dq,
    dl,
    dr,
    qg,
    lg,
    uq,
    ur,
    ku,
    vu,
    lat,
    rope,
    op,
    absorbed,
    rx1,
    rx2,
    tx3,
    rx3,
    rxy,
    rxz,
    rx6,
    lengths,
    inverse,
    load_sem,
    send_sem,
    recv_sem,
):
    Z = K // Y
    B, D = hidden.shape[0], hidden.shape[1] * T
    QR, KR, DR = dq.shape[1], dl.shape[1], dr.shape[0]
    DN, DV = uq.shape[1], vu.shape[1]
    span = lat.shape[1]
    cols = op.shape[2]
    k = lax.axis_index("kv")
    t = lax.axis_index("tp")
    z, y = k // Y, lax.rem(k, Y)
    factor = 1.0 / math.sqrt(DN + DR)

    def peer(axis, i):
        if axis == "x":
            return (k, lax.rem(t + i, T))
        if axis == "y":
            return (z * Y + lax.rem(y + i, Y), t)
        return (lax.rem(z + i, Z) * Y + y, t)

    barrier = pltpu.get_barrier_semaphore()
    for i in RING:
        for axis in "yzx":
            pl.semaphore_signal(barrier, inc=1, device_id=peer(axis, i), device_id_type=MESH)

    pairs = (
        (hidden_h, hidden), (gain_h, gain), (dq_h, dq), (dl_h, dl), (dr_h, dr),
        (op_h, op.at[z, y]), (lengths_h, lengths), (inverse_h, inverse),
        (uq_h, uq), (ku_h, ku), (ur_h, ur.at[pl.ds(0, DR)]), (qg_h, qg), (lg_h, lg), (vu_h, vu),
        (lat_h, lat), (rope_h, rope.at[:, pl.ds(0, DR)]), (rope_h, rope.at[:, pl.ds(DR, DR)]),
    )
    loads = [pltpu.make_async_copy(a, b, load_sem.at[i]) for i, (a, b) in enumerate(pairs)]
    for load in loads:
        load.start()

    def send(phase, axis, src, dst):
        for i in RING:
            pltpu.make_async_remote_copy(
                src_ref=src(i),
                dst_ref=dst,
                send_sem=send_sem.at[phase],
                recv_sem=recv_sem.at[phase],
                device_id=peer(axis, i),
                device_id_type=MESH,
            ).start()

    def drain(buffer, sem):
        pltpu.make_async_copy(buffer.at[pl.ds(0, 7)], buffer.at[pl.ds(0, 7)], sem).wait()

    for load in loads[:5]:
        load.wait()
    floats = hidden[...].astype(F32)
    scaled = (floats * gain[...]).astype(BF16)
    squares = jnp.sum(floats * floats, axis=1, keepdims=True)
    low = rx1.at[t]
    low[...] = jnp.concatenate(
        [
            dot(scaled, dq[...]),
            dot(scaled, dl[...]),
            dot_nt(scaled, dr[...]),
            jnp.broadcast_to(squares, (B, rx1.shape[2] - QR - KR - DR)),
        ],
        axis=1,
    ).astype(BF16)
    loads[5].wait()
    pl.semaphore_wait(barrier, 21)
    send(0, "x", lambda i: rx1.at[t], rx1.at[t])
    send(6, "y", lambda i: op.at[z, y], op.at[z, y])

    for load in loads[6:]:
        load.wait()
    absorbed[...] = dot_nt(uq[...], ku[...]).astype(BF16)
    half = DR // 2
    turned = ur[:DR].astype(F32)
    ur[DR:] = jnp.concatenate([-turned[half:], turned[:half]], axis=0).astype(BF16)
    seq = iota((B, DR), 0)
    position = jnp.zeros((B, DR), F32)
    for b in range(B):
        position = jnp.where(seq == b, lengths[b].astype(F32), position)
    sine, cosine = sin_cos(position * inverse[...])
    rotary = jnp.concatenate([cosine, sine], axis=1)
    rows = lax.rem(iota((T * B, span), 0), B)
    limit = jnp.zeros((T * B, span), jnp.int32)
    for b in range(B):
        limit = jnp.where(rows == b, lengths[b], limit)
    usable = iota((T * B, span), 1) + (k * T + t) * span < limit

    drain(rx1, recv_sem.at[0])
    total = rx1[0].astype(F32)
    for i in range(1, T):
        total = total + rx1[i].astype(F32)
    inv2 = 1.0 / (total[:, QR + KR + DR : QR + KR + DR + 1] / D + EPSILON)
    inv = jnp.sqrt(inv2)

    def low_norm(v, g):
        mean = jnp.mean(v * v, axis=-1, keepdims=True) * inv2
        return v * (inv * lax.rsqrt(mean + EPSILON)) * g

    query_normed = low_norm(total[:, :QR], qg[...]).astype(BF16)
    own_latent = dot(query_normed, absorbed[...])
    own_rope = dot_nt(query_normed, ur[...]) * rotary
    query = jnp.concatenate([own_latent, own_rope], axis=1)
    rx2[t] = query.astype(BF16)
    send(1, "x", lambda i: rx2.at[t], rx2.at[t])

    drain(op.at[z], recv_sem.at[6])
    send(7, "z", lambda i: op.at[z], op.at[z])
    latent_new = low_norm(total[:, QR : QR + KR], lg[...]).astype(BF16)
    rope_low = total[:, QR + KR : QR + KR + DR] * inv
    swapped = jnp.concatenate([-rope_low[:, half:], rope_low[:, :half]], axis=1)
    rope_new = (rope_low * cosine + swapped * sine).astype(BF16).astype(F32)
    rope_new = jnp.concatenate([rope_new, rope_new], axis=1)
    rounded = query.astype(BF16).astype(F32)
    new_score = (
        jnp.sum(rounded[:, :KR] * latent_new.astype(F32), axis=1, keepdims=True)
        + jnp.sum(rounded[:, KR:] * rope_new, axis=1, keepdims=True)
    ) * factor
    new_value = dot(latent_new, vu[...])

    drain(rx2, recv_sem.at[1])
    queries = rx2[...].astype(F32).reshape(T * B, rx2.shape[2]).astype(BF16)
    scores = jnp.zeros((T * B, span), F32)
    for b in range(B):
        part = dot_nt(queries[:, :KR], lat[b]) + dot(queries[:, KR:], rope[b])
        scores = jnp.where(rows == b, part, scores)
    scores = jnp.where(usable, scores * factor, -1e30)
    top = jnp.max(scores, axis=1, keepdims=True).astype(BF16).astype(F32)
    weights = jnp.where(usable, jnp.exp(scores - top), 0.0)
    mass = jnp.sum(weights, axis=1, keepdims=True)
    summed = jnp.zeros((T * B, KR), F32)
    for b in range(B):
        summed = summed + dot(jnp.where(rows == b, weights, 0.0).astype(BF16), lat[b])
    mark = iota((T * B, 128), 1)
    tail = jnp.where(mark == 0, top, mass)
    block = jnp.concatenate([summed, tail], axis=1)
    tx3[...] = block.reshape(T, B, KR + 128).astype(BF16)
    send(2, "x", lambda i: tx3.at[lax.rem(t + i, T)], rx3.at[t])
    rx3[t] = tx3[t]
    drain(rx3, recv_sem.at[2])

    mark = iota((B, 128), 1)

    def combine(buffer, n):
        parts = buffer[...].astype(F32)
        tops = parts[:, :, n : n + 1]
        highest = jnp.max(tops, axis=0)
        scale = jnp.exp(tops - highest)
        return jnp.sum(parts * scale, axis=0), highest

    def share(phase, axis, buffer, slot, value, mass, highest):
        tail = jnp.where(mark == 0, highest, mass)
        buffer[slot] = jnp.concatenate([value, tail], axis=1).astype(BF16)
        send(phase, axis, lambda i: buffer.at[slot], buffer.at[slot])
        drain(buffer, recv_sem.at[phase])

    total, highest = combine(rx3, KR)
    value = dot(total[:, :KR].astype(BF16), vu[...])
    share(3, "y", rxy, y, value, total[:, KR:], highest)
    total, highest = combine(rxy, DV)
    share(4, "z", rxz, z, total[:, :DV], total[:, DV:], highest)
    total, highest = combine(rxz, DV)
    final = jnp.maximum(highest, new_score)
    old = jnp.exp(highest - final)
    fresh = jnp.exp(new_score - final)
    mass = total[:, DV + 1 : DV + 2] * old + fresh
    value = ((total[:, :DV] * old + new_value * fresh) / mass).astype(BF16)

    drain(op, recv_sem.at[7])
    everything = op[...].reshape(K * cols, DV)
    own = jnp.concatenate([op[z, y], jnp.zeros((128 - cols, DV), BF16)], axis=0)
    rx6[t] = jnp.concatenate([dot_nt(value, everything), dot_nt(value, own)], axis=1).astype(BF16)
    send(5, "x", lambda i: rx6.at[t], rx6.at[t])
    drain(rx6, recv_sem.at[5])
    total = rx6[0].astype(F32)
    for i in range(1, T):
        total = total + rx6[i].astype(F32)
    full = total[:, : K * cols]
    mean = jnp.mean(full * full, axis=1, keepdims=True)
    out[...] = total[:, K * cols : K * cols + cols] * lax.rsqrt(mean + EPSILON)

    for phase, buffer in enumerate((rx1, rx2, rx3, rxy, rxz, rx6, op.at[z], op)):
        drain(buffer, send_sem.at[phase])


def shards(
    K, T, hidden_in, input_gain, down_query, down_latent, down_rope, query_gain, latent_gain,
    up_query, up_rope, key_up, value_up, out_proj, output_gain, latent_cache, rope_cache, lengths,
):
    B = hidden_in.shape[0]
    QR, Hd, DN = up_query.shape
    KR, DR, DV = key_up.shape[0], up_rope.shape[2], value_up.shape[2]
    span, cols = latent_cache.shape[1], out_proj.shape[1]
    steps = np.arange(0, DR, 2, dtype=np.float64) / DR
    inverse = np.tile((1.0 / THETA**steps).astype(np.float32), 2)[None, :]
    flat = lambda w: w.reshape(w.shape[0] * w.shape[1], w.shape[2])
    row = lambda v: v.reshape(1, v.shape[0])
    arrays = (
        hidden_in, row(input_gain), down_query, down_latent, down_rope.T, row(query_gain),
        row(latent_gain), flat(up_query), flat(up_rope.transpose(1, 2, 0)), flat(key_up),
        flat(value_up), out_proj.T, latent_cache, rope_cache.transpose(0, 2, 1),
    )
    vm = lambda *shape: pltpu.VMEM(shape, BF16)
    low = -(-(QR + KR + DR + 1) // 128) * 128
    dma = pltpu.SemaphoreType.DMA
    scratch = [
        vm(*hidden_in.shape),
        pltpu.VMEM((1, input_gain.shape[0]), F32),
        vm(*down_query.shape),
        vm(*down_latent.shape),
        vm(DR, down_rope.shape[0]),
        pltpu.VMEM((1, QR), F32),
        pltpu.VMEM((1, KR), F32),
        vm(QR, DN),
        vm(2 * DR, QR),
        vm(KR, DN),
        vm(KR, DV),
        vm(B, span, KR),
        vm(B, 2 * DR, span),
        vm(K // Y, Y, cols, DV),
        vm(QR, KR),
        vm(T, B, low),
        vm(T, B, KR + 128),
        vm(T, B, KR + 128),
        vm(T, B, KR + 128),
        vm(Y, B, DV + 128),
        vm(K // Y, B, DV + 128),
        vm(T, B, K * cols + 128),
        pltpu.SMEM(lengths.shape, lengths.dtype),
        pltpu.VMEM(inverse.shape, F32),
        dma((len(arrays) + 3,)),
        dma((8,)),
        dma((8,)),
    ]
    normal = pl.pallas_call(
        functools.partial(kernel, K, T),
        out_shape=jax.ShapeDtypeStruct((B, cols), F32),
        in_specs=[pl.BlockSpec(memory_space=pl.ANY)] * (len(arrays) + 2),
        out_specs=pl.BlockSpec(memory_space=pltpu.VMEM),
        scratch_shapes=scratch,
        compiler_params=pltpu.CompilerParams(collective_id=0, has_side_effects=True),
    )(lengths, jnp.asarray(inverse), *arrays)
    return (normal * row(output_gain)).astype(BF16)


def solution(mesh):
    in_specs = (
        P(None, "tp"),
        P("tp"),
        P("tp", None),
        P("tp", None),
        P("tp", None),
        P(),
        P(),
        P(None, "tp", None),
        P(None, "tp", None),
        P(None, "tp", None),
        P(None, "tp", None),
        P("tp", "kv"),
        P("kv"),
        P(None, ("kv", "tp"), None),
        P(None, ("kv", "tp"), None),
        P(),
    )
    body = functools.partial(shards, mesh.shape["kv"], mesh.shape["tp"])
    return jax.shard_map(body, mesh=mesh, in_specs=in_specs, out_specs=P(None, "kv"), check_vma=False)
```

time: 79.8 us -> 42.1 us (0.53)
  Pallas kernels: 78.4 us -> 40.7 us
    pallas_call x1, Pallas kernels: 78.4 us -> 40.7 us  [shards(): pl.pallas_call(functools.partial(kernel, K, T), out_shape=jax.ShapeDtypeS...]
where the time goes in v1:
time: 42.1 us; the launch traced here: 42 us
  Pallas kernels  40.7 us (97%)
  other arithmetic  1.25 us (3%)
    pallas_call x1, Pallas kernels, shards(): pl.pallas_call(functools.partial(kernel, K, T), out_shape=jax.ShapeDtypeS...  40.7 us
    convert_element_type x1, other arithmetic, shards(): return (normal * row(output_gain)).astype(BF16)  1.25 us

profile of v1, /device:TPU:1, one launch (start us, length us, event | category | flops | bytes accessed | tf_op | source)
XLA Modules:
  0.0 42.0 jit_solution(5032068012826186160)
XLA Ops:
  0.0 0.0 copy-start
  0.0 40.7 %shard_map.163 = f32[8,16]{1,0:T(8,128)} custom-call(s32[8]{0:T(128)} %lengths_h.1, f32[1,64]{1,0:T(1,128)} %constant.2.clone.inverse_h, bf16[8,128]{1,0:T(8,128)(2,1)} %hidden_h.1, f32[1,128]{1,0:T(1,128)} %bitcast.21, bf16[128,256]{1,0:T(8,128)(2,1)} %dq_h.1, bf16[128,256]{1,0:T(8,128)(2,1)} %dl_h.1, bf16[64,128]{1,0:T(8,128)(2,1)} %bitcast.17, ...), custom_call_target="tpu_custom_call" | custom-call | tf_op jit(solution)/shard_map/pallas_call | solution.py:326
  40.7 0.0 copy-done
  40.7 1.3 %multiply_convert_fusion = bf16[8,16]{1,0:T(8,128)(2,1)} fusion(f32[8,16]{1,0:T(8,128)} %shard_map.163, f32[16]{0:T(128)S(1)} %copy-done), kind=kLoop, calls=%fused_computation | loop fusion | flops 256 | bytes 832 | tf_op jit(solution)/shard_map/convert_element_type | solution.py:334
Async XLA Ops:
  0.0 40.7 %copy-start = (f32[16]{0:T(128)S(1)}, f32[16]{0:T(128)}, u32[]{:S(2)}) copy-start(f32[16]{0:T(128)} %param.29) | copy-start | bytes 196
